TPU v7x, 32 devices: a whole 2x2x4 slice. The times are simulated.
32 devices in a mesh: sp: 4 (over z), tp: 4 (over y, x), dp: 2 (over core).
Axes of the slice: x: 2, y: 2, z: 4, core: 2. Of those that a mesh axis runs over, the one named last changes fastest.
Arguments:
- latent_in: bfloat16 [3072, 2048], P(('dp', 'sp', 'tp')), parts along dimension 0, may hold values from -6 to 6
- condition: bfloat16 [4096], P(('dp', 'sp')), parts along dimension 0, may hold values from -8 to 8
- context_latent: bfloat16 [1024, 256], P(('dp', 'sp')), parts along dimension 0, may hold values from -6 to 6
- context_rope: bfloat16 [1024, 64], P(('dp', 'sp')), parts along dimension 0, may hold values from -6 to 6
- shift_weight: bfloat16 [2048, 2048], P('sp', 'tp'), may hold values from -0.125 to 0.125
- scale_weight: bfloat16 [2048, 2048], P('sp', 'tp'), may hold values from -0.125 to 0.125
- gate_weight: bfloat16 [2048, 2048], P('sp', 'tp'), may hold values from -0.125 to 0.125
- norm_gain: float32 [2048], replicated, may hold values from 0.1 to 1.9
- down_query: bfloat16 [2048, 512], replicated, may hold values from -0.125 to 0.125
- down_latent: bfloat16 [2048, 256], replicated, may hold values from -0.125 to 0.125
- down_rope: bfloat16 [2048, 64], replicated, may hold values from -0.125 to 0.125
- query_gain: float32 [512], replicated, may hold values from 0.5 to 60
- latent_gain: float32 [256], replicated, may hold values from 0.1 to 1.9
- up_query: bfloat16 [512, 1536], P(None, 'tp'), may hold values from -0.25 to 0.25
- up_key: bfloat16 [256, 1024], P(None, 'tp'), may hold values from -0.375 to 0.375
- up_value: bfloat16 [256, 1024], P(None, 'tp'), may hold values from -0.375 to 0.375
- context_bias: float32 [8], P('tp'), may hold values from 1 to 2.5
- out_weight: bfloat16 [1024, 2048], replicated, may hold values from -3 to 3
Outputs:
- mixed_out: bfloat16 [3072, 2048], P(('dp', 'sp', 'tp')), parts along dimension 0
There are 2 independent parts, one for each index of `dp`. A program takes and returns all parts, laid end to end along the dimension named above; an argument that names none is the same for every part. Nothing has to cross between parts.
All inputs are finite; a program needn't handle non-finite values.
Results may differ from a plain program's by a relative error of at most 0.039.
The roundings to bfloat16 on the way count: a program that leaves them out, or rounds other values in their place, can miss the bound.
Values may be sent and summed in bfloat16 or wider, within the bound.
A program may use at most 128 MiB of HBM per device.

v0:
```python
import jax
import jax.numpy as jnp
from jax import lax
from jax.sharding import PartitionSpec as P

QK_NOPE = 128
QK_ROPE = 64
V_HEAD = 128
GRID_W = 64
epsilon = 1e-06
rope_base = 10000.0
block_limit = 2048


def rms_scaled(values, gain_vec):
    mean_sq = jnp.mean(values * values, axis=-1, keepdims=True)
    return values * lax.rsqrt(mean_sq + epsilon) * gain_vec


def rope_tables(positions, rope_width):
    freq_count = rope_width // 4
    inverse = rope_base ** (-jnp.arange(freq_count, dtype=jnp.float32) / freq_count)
    grid_row = (positions // GRID_W).astype(jnp.float32)
    grid_col = (positions % GRID_W).astype(jnp.float32)
    row_angle = grid_row[:, None] * inverse
    col_angle = grid_col[:, None] * inverse
    angles = jnp.concatenate([row_angle, row_angle, col_angle, col_angle], axis=-1)
    return (jnp.cos(angles), jnp.sin(angles))


def rope_turn(values, cosine_table, sine_table):
    part_one, part_two, part_three, part_four = jnp.split(values, 4, axis=-1)
    turned = jnp.concatenate([-part_two, part_one, -part_four, part_three], axis=-1)
    return values * cosine_table + turned * sine_table


def attend(attn_state, query_nope, query_rope, keys_nope, values_in, keys_rope, bias_col):
    score_scale = (query_nope.shape[-1] + query_rope.shape[-1]) ** (-0.5)
    scores = jnp.einsum("thd,khd->htk", query_nope, keys_nope, preferred_element_type=jnp.float32)
    scores = scores + jnp.einsum(
        "thr,kr->htk", query_rope, keys_rope, preferred_element_type=jnp.float32
    )
    scores = scores * score_scale + bias_col
    run_max, run_total, run_acc = attn_state
    new_max = jnp.maximum(run_max, jnp.max(scores, axis=-1))
    shrink = jnp.exp(run_max - new_max)
    weights = jnp.exp(scores - new_max[:, :, None])
    new_total = run_total * shrink + jnp.sum(weights, axis=-1)
    new_acc = run_acc * shrink[:, :, None] + jnp.einsum(
        "htk,khd->htd", weights.astype(jnp.bfloat16), values_in, preferred_element_type=jnp.float32
    )
    return (new_max, new_total, new_acc)


def over_blocks(attn_state, arrays, handle):
    row_count = arrays[0].shape[0]
    block_rows = 1
    for candidate in range(min(row_count, block_limit), 0, -1):
        if row_count % candidate == 0:
            block_rows = candidate
            break
    block_count = row_count // block_rows
    if block_count == 1:
        return handle(attn_state, arrays)
    stacked = tuple(
        (array_in.reshape((block_count, block_rows) + array_in.shape[1:]) for array_in in arrays)
    )

    def one_turn(inner_state, pieces):
        return (handle(inner_state, pieces), None)

    return lax.scan(one_turn, attn_state, stacked)[0]


def on_device(
    latent_in,
    condition,
    context_latent,
    context_rope,
    shift_weight,
    scale_weight,
    gate_weight,
    norm_gain,
    down_query,
    down_latent,
    down_rope,
    query_gain,
    latent_gain,
    up_query,
    up_key,
    up_value,
    context_bias,
    out_weight,
):
    activated = jax.nn.silu(condition.astype(jnp.float32)).astype(jnp.bfloat16)
    partials = jnp.stack(
        [
            jnp.dot(activated, weight_in, preferred_element_type=jnp.float32)
            for weight_in in (shift_weight, scale_weight, gate_weight)
        ]
    )
    summed = lax.psum(partials, "sp")
    modulation = lax.all_gather(summed, "tp", axis=1, tiled=True)
    shift_vec = modulation[0]
    scale_vec = modulation[1]
    gate_vec = modulation[2]
    residual_in = latent_in.astype(jnp.float32)
    normed = (rms_scaled(residual_in, norm_gain) * (1.0 + scale_vec) + shift_vec).astype(
        jnp.bfloat16
    )
    query_low = rms_scaled(
        jnp.dot(normed, down_query, preferred_element_type=jnp.float32), query_gain
    ).astype(jnp.bfloat16)
    latent_low = rms_scaled(
        jnp.dot(normed, down_latent, preferred_element_type=jnp.float32), latent_gain
    ).astype(jnp.bfloat16)
    local_rows = latent_in.shape[0]
    first_row = (lax.axis_index("sp") * lax.axis_size("tp") + lax.axis_index("tp")) * local_rows
    own_positions = first_row + jnp.arange(local_rows, dtype=jnp.int32)
    own_cosine, own_sine = rope_tables(own_positions, QK_ROPE)
    rope_keys = rope_turn(
        jnp.dot(normed, down_rope, preferred_element_type=jnp.float32), own_cosine, own_sine
    ).astype(jnp.bfloat16)
    query_group, latent_group, rope_group = (
        lax.all_gather(query_low, "tp", axis=0, tiled=True),
        lax.all_gather(latent_low, "tp", axis=0, tiled=True),
        lax.all_gather(rope_keys, "tp", axis=0, tiled=True),
    )
    group_rows = query_group.shape[0]
    group_positions = lax.axis_index("sp") * group_rows + jnp.arange(group_rows, dtype=jnp.int32)
    group_cosine, group_sine = rope_tables(group_positions, QK_ROPE)
    head_count = up_key.shape[1] // QK_NOPE
    queries = jnp.dot(query_group, up_query, preferred_element_type=jnp.float32).reshape(
        group_rows, head_count, QK_NOPE + QK_ROPE
    )
    query_nope = queries[:, :, :QK_NOPE].astype(jnp.bfloat16)
    query_rope = rope_turn(
        queries[:, :, QK_NOPE:], group_cosine[:, None, :], group_sine[:, None, :]
    ).astype(jnp.bfloat16)
    context_all, context_keys_rope = (
        lax.all_gather(context_latent, "sp", axis=0, tiled=True),
        lax.all_gather(context_rope, "sp", axis=0, tiled=True),
    )
    context_count = context_all.shape[0]
    context_nope = (
        jnp.dot(context_all, up_key, preferred_element_type=jnp.float32)
        .astype(jnp.bfloat16)
        .reshape(context_count, head_count, QK_NOPE)
    )
    context_values = (
        jnp.dot(context_all, up_value, preferred_element_type=jnp.float32)
        .astype(jnp.bfloat16)
        .reshape(context_count, head_count, V_HEAD)
    )
    start_state = (
        jnp.full((head_count, group_rows), -jnp.inf, jnp.float32),
        jnp.zeros((head_count, group_rows), jnp.float32),
        jnp.zeros((head_count, group_rows, V_HEAD), jnp.float32),
    )
    bias_col = context_bias[:, None, None]

    def context_step(inner_state, pieces):
        return attend(
            inner_state, query_nope, query_rope, pieces[0], pieces[1], pieces[2], bias_col
        )

    attn_state = over_blocks(
        start_state, (context_nope, context_values, context_keys_rope), context_step
    )
    own_nope = jnp.dot(latent_group, up_key, preferred_element_type=jnp.float32).astype(
        jnp.bfloat16
    )
    own_values = jnp.dot(latent_group, up_value, preferred_element_type=jnp.float32).astype(
        jnp.bfloat16
    )

    def expanded_step(inner_state, pieces):
        piece_rows = pieces[0].shape[0]
        return attend(
            inner_state,
            query_nope,
            query_rope,
            pieces[0].reshape(piece_rows, head_count, QK_NOPE),
            pieces[1].reshape(piece_rows, head_count, V_HEAD),
            pieces[2],
            0.0,
        )

    attn_state = over_blocks(
        attn_state,
        (
            lax.all_gather(own_nope, "sp", axis=0, tiled=True),
            lax.all_gather(own_values, "sp", axis=0, tiled=True),
            lax.all_gather(rope_group, "sp", axis=0, tiled=True),
        ),
        expanded_step,
    )
    attended = (attn_state[2] / attn_state[1][:, :, None]).astype(jnp.bfloat16)
    attended = attended.transpose(1, 0, 2).reshape(group_rows, head_count * V_HEAD)
    token_major = lax.all_to_all(attended, "tp", split_axis=0, concat_axis=1, tiled=True)
    mixed = jnp.dot(token_major, out_weight, preferred_element_type=jnp.float32)
    return (residual_in + gate_vec * mixed).astype(jnp.bfloat16)


def solution(mesh):
    in_specs = (
        P(("dp", "sp", "tp"), None),
        P(("dp", "sp")),
        P(("dp", "sp"), None),
        P(("dp", "sp"), None),
        P("sp", "tp"),
        P("sp", "tp"),
        P("sp", "tp"),
        P(),
        P(),
        P(),
        P(),
        P(),
        P(),
        P(None, "tp"),
        P(None, "tp"),
        P(None, "tp"),
        P("tp"),
        P(),
    )
    out_specs = P(("dp", "sp", "tp"), None)
    return jax.shard_map(
        on_device, mesh=mesh, in_specs=in_specs, out_specs=out_specs, check_vma=False
    )
```

profile of v0, /device:TPU:0, one launch (start us, length us, event | category | flops | bytes accessed | tf_op | source)
XLA Modules:
  0.0 158.6 jit_solution(2897633564219635338)
XLA Ops:
  0.6 0.7 fusion.54
  1.3 1.2 fusion.72
  2.6 1.2 fusion.73
  3.8 1.3 fusion.74
  5.1 13.8 %psum.7 = f32[3,512]{1,0:T(4,128)S(1)} all-reduce(f32[3,512]{1,0:T(4,128)S(1)} %pad_maximum_fusion.2), channel_id=1, replica_groups=mesh['sp'=4,'tp'=4,'dp'=2] {'sp'}, use_global_device_ids=true, to_apply=%region_0.1 | all-reduce | flops 1536 | bytes 12288 | tf_op jit(solution)/shard_map/psum | solution.py:102
  18.9 8.2 %all_gather.27 = f32[3,2048]{1,0:T(4,128)S(1)} all-gather(f32[3,512]{1,0:T(4,128)S(1)} %psum.7), channel_id=1, replica_groups=mesh['sp'=4,'tp'=4,'dp'=2] {'tp'}, dimensions={1}, use_global_device_ids=true | all-gather | bytes 30720 | tf_op jit(solution)/shard_map/all_gather | solution.py:103
  27.1 1.2 fusion.26
  28.4 1.9 %multiply_reduce_fusion.1 = (f32[96]{0:T(128)S(1)}, f32[96,256]{1,0:T(8,128)S(1)}) fusion(bf16[2048,256]{1,0:T(8,128)(2,1)} %param.27, bf16[96,2048]{1,0:T(8,128)(2,1)} %param.18, f32[2048]{0:T(1024)S(1)} %bitcast.119, f32[2048]{0:T(1024)S(1)} %bitcast.122, f32[2048]{0:T(1024)} %param.25, f32[96]{0:T(128)S(1)} %add_rsqrt_fusion.2), kind=kOutput, calls=%fused_computation.50 | convolution fusion | flops 101892000 | bytes 1565440 | tf_op jit(solution)/shard_map/dot_general | solution.py:115
  30.3 8.7 %all_gather.31 = bf16[384,256]{1,0:T(8,128)(2,1)S(1)} all-gather(bf16[96,256]{1,0:T(8,128)(2,1)S(1)} %multiply_convert_fusion.1), channel_id=1, replica_groups=mesh['sp'=4,'tp'=4,'dp'=2] {'tp'}, dimensions={0}, use_global_device_ids=true | all-gather | bytes 245760 | tf_op jit(solution)/shard_map/all_gather | solution.py:126
  39.1 13.8 %all_gather.29 = bf16[512,256]{1,0:T(8,128)(2,1)S(1)} all-gather(bf16[128,256]{1,0:T(8,128)(2,1)S(1)} %copy-done.12), channel_id=1, replica_groups=mesh['sp'=4,'tp'=4,'dp'=2] {'sp'}, dimensions={0}, use_global_device_ids=true | all-gather | bytes 327680 | tf_op jit(solution)/shard_map/all_gather | solution.py:141
  52.9 0.9 convolution_convert_fusion.3
  54.0 1.0 convolution_convert_fusion
  56.0 8.5 %all_gather.28 = bf16[384,512]{1,0:T(8,128)(2,1)S(1)} all-gather(bf16[96,512]{1,0:T(8,128)(2,1)S(1)} %multiply_convert_fusion), channel_id=1, replica_groups=mesh['sp'=4,'tp'=4,'dp'=2] {'tp'}, dimensions={0}, use_global_device_ids=true | all-gather | bytes 491520 | tf_op jit(solution)/shard_map/all_gather | solution.py:125
  65.0 0.7 slice_negate_fusion.1
  66.3 1.3 fusion.62
  67.6 0.6 copy-done.11
  68.9 0.7 broadcast_multiply_fusion.3
  69.6 0.9 fusion.47
  70.5 8.2 %all-gather = bf16[4,96,64]{1,2,0:T(8,128)(2,1)S(1)} all-gather(bf16[1,96,64]{1,2,0:T(8,128)(2,1)S(1)} %fusion.47), channel_id=1, replica_groups=mesh['sp'=4,'tp'=4,'dp'=2] {'tp'}, dimensions={0}, use_global_device_ids=true | all-gather | bytes 61440 | tf_op jit(solution)/shard_map/all_gather | solution.py:127
  78.7 0.7 copy.48
  79.4 1.6 reshape.254
  81.0 14.6 %all_gather.34 = bf16[1536,64]{0,1:T(8,128)(2,1)S(1)} all-gather(bf16[384,64]{0,1:T(8,128)(2,1)} %reshape.254), channel_id=1, replica_groups=mesh['sp'=4,'tp'=4,'dp'=2] {'sp'}, dimensions={0}, use_global_device_ids=true | all-gather | bytes 245760 | tf_op jit(solution)/shard_map/all_gather | solution.py:194
  95.6 16.9 %all_gather.32 = bf16[1536,256]{1,0:T(8,128)(2,1)S(1)} all-gather(bf16[384,256]{1,0:T(8,128)(2,1)} %convolution_convert_fusion.3), channel_id=1, replica_groups=mesh['sp'=4,'tp'=4,'dp'=2] {'sp'}, dimensions={0}, use_global_device_ids=true | all-gather | bytes 983040 | tf_op jit(solution)/shard_map/all_gather | solution.py:192
  112.9 12.2 %all_gather.30 = bf16[512,64]{0,1:T(8,128)(2,1)S(1)} all-gather(bf16[128,64]{0,1:T(8,128)(2,1)S(1)} %copy-done.13), channel_id=1, replica_groups=mesh['sp'=4,'tp'=4,'dp'=2] {'sp'}, dimensions={0}, use_global_device_ids=true | all-gather | bytes 81920 | tf_op jit(solution)/shard_map/all_gather | solution.py:142
  125.4 0.8 fusion.39
  126.3 1.0 fusion.71
  128.3 15.6 %all_gather.35 = bf16[1536,256]{1,0:T(8,128)(2,1)S(1)} all-gather(bf16[384,256]{1,0:T(8,128)(2,1)S(1)} %convolution_convert_fusion.2), channel_id=1, replica_groups=mesh['sp'=4,'tp'=4,'dp'=2] {'sp'}, dimensions={0}, use_global_device_ids=true | all-gather | bytes 983040 | tf_op jit(solution)/shard_map/all_gather | solution.py:193
  143.8 0.8 fusion.1
  144.8 0.7 fusion.19
  145.5 0.9 fusion.23
  146.8 8.1 %all_to_all.19 = bf16[4,96,256]{2,1,0:T(8,128)(2,1)S(1)} all-to-all(bf16[4,96,256]{2,1,0:T(8,128)(2,1)S(1)} %all_to_all.14), channel_id=1, replica_groups=mesh['sp'=4,'tp'=4,'dp'=2] {'tp'}, dimensions={0} | all-to-all | bytes 393216 | tf_op jit(solution)/shard_map/all_to_all | solution.py:200
  154.9 3.8 %fusion.7 = bf16[96,2048]{1,0:T(8,128)(2,1)} fusion(bf16[96,1024]{1,0:T(8,128)(2,1)S(1)} %bitcast.116, bf16[1024,2048]{1,0:T(8,128)(2,1)} %param.35, bf16[96,2048]{1,0:T(8,128)(2,1)S(1)} %copy-done.1, f32[2048]{0:T(1024)S(1)} %bitcast.118), kind=kOutput, calls=%fused_computation.9 | convolution fusion | flops 403439616 | bytes 5185536 | tf_op jit(solution)/shard_map/dot_general | solution.py:201
  (72 shorter events, 5.8 us)
Async XLA Ops:
  0.0 55.3 %copy-start = (bf16[2048,512]{1,0:T(8,128)(2,1)S(1)}, bf16[2048,512]{1,0:T(8,128)(2,1)}, u32[]{:S(2)}) copy-start(bf16[2048,512]{1,0:T(8,128)(2,1)} %param.26) | copy-start | bytes 6291460
  0.0 30.2 %copy-start.19 = (f32[256]{0:T(256)S(1)}, f32[256]{0:T(256)}, u32[]{:S(2)}) copy-start(f32[256]{0:T(256)} %param.30) | copy-start | bytes 3076
  0.0 39.0 %copy-start.12 = (bf16[128,256]{1,0:T(8,128)(2,1)S(1)}, bf16[128,256]{1,0:T(8,128)(2,1)}, u32[]{:S(2)}) copy-start(bf16[128,256]{1,0:T(8,128)(2,1)} %param.20) | copy-start | bytes 196612
  1.3 51.5 %copy-start.3 = (bf16[256,256]{1,0:T(8,128)(2,1)S(1)}, bf16[256,256]{1,0:T(8,128)(2,1)}, u32[]{:S(2)}) copy-start(bf16[256,256]{1,0:T(8,128)(2,1)} %param.32) | copy-start | bytes 393220
  3.8 50.2 %copy-start.4 = (bf16[256,256]{1,0:T(8,128)(2,1)S(1)}, bf16[256,256]{1,0:T(8,128)(2,1)}, u32[]{:S(2)}) copy-start(bf16[256,256]{1,0:T(8,128)(2,1)} %param.33) | copy-start | bytes 393220
  27.1 28.1 %copy-start.14 = (f32[1,2048]{1,0:T(1,128)}, f32[1,2048]{1,0:T(1,128)S(1)}, u32[]{:S(2)}) copy-start(f32[1,2048]{1,0:T(1,128)S(1)} %get-tuple-element.15) | copy-start | bytes 24580
  27.1 27.9 %copy-start.5 = (bf16[256,256]{1,0:T(8,128)(2,1)S(1)}, bf16[256,256]{1,0:T(8,128)(2,1)}, u32[]{:S(2)}) copy-start(bf16[256,256]{1,0:T(8,128)(2,1)} %param.33) | copy-start | bytes 393220
  28.3 26.9 %copy-start.22 = (f32[96]{0:T(128)}, f32[96]{0:T(128)S(1)}, u32[]{:S(2)}) copy-start(f32[96]{0:T(128)S(1)} %add_rsqrt_fusion.2) | copy-start | bytes 1156
  28.3 26.9 %copy-start.1 = (bf16[96,2048]{1,0:T(8,128)(2,1)S(1)}, bf16[96,2048]{1,0:T(8,128)(2,1)}, u32[]{:S(2)}) copy-start(bf16[96,2048]{1,0:T(8,128)(2,1)} %param.18) | copy-start | bytes 1179652
  28.4 26.9 %copy-start.21 = (f32[2048]{0:T(1024)S(1)}, f32[2048]{0:T(1024)}, u32[]{:S(2)}) copy-start(f32[2048]{0:T(1024)} %param.25) | copy-start | bytes 24580
  53.7 2.2 %copy-start.17 = (f32[512]{0:T(512)S(1)}, f32[512]{0:T(512)}, u32[]{:S(2)}) copy-start(f32[512]{0:T(512)} %param.29) | copy-start | bytes 6148
  54.0 10.5 %copy-start.6 = (bf16[512,384]{1,0:T(8,128)(2,1)S(1)}, bf16[512,384]{1,0:T(8,128)(2,1)}, u32[]{:S(2)}) copy-start(bf16[512,384]{1,0:T(8,128)(2,1)} %param.31) | copy-start | bytes 1179652
  67.6 0.6 copy-start.11
  70.5 54.6 %copy-start.15 = (f32[384]{0:T(512)S(1)}, f32[384]{0:T(512)}, u32[]{:S(2)}) copy-start(f32[384]{0:T(512)} %get-tuple-element.33) | copy-start | bytes 4612
  70.5 54.6 %copy-start.16 = (f32[384]{0:T(512)S(1)}, f32[384]{0:T(512)}, u32[]{:S(2)}) copy-start(f32[384]{0:T(512)} %get-tuple-element.34) | copy-start | bytes 4612
  81.0 31.9 %copy-start.13 = (bf16[128,64]{0,1:T(8,128)(2,1)S(1)}, bf16[128,64]{0,1:T(8,128)(2,1)}, u32[]{:S(2)}) copy-start(bf16[128,64]{0,1:T(8,128)(2,1)} %param.21) | copy-start | bytes 49156
  81.0 44.1 %copy-start.18 = (f32[16]{0:T(128)S(1)}, f32[16]{0:T(128)}, u32[]{:S(2)}) copy-start(f32[16]{0:T(128)} %multiply_power_fusion) | copy-start | bytes 196
  81.0 44.4 %copy-start.7 = (f32[384,2,16]{0,2,1:T(8,128)S(1)}, f32[384,2,16]{0,2,1:T(8,128)}, u32[]{:S(2)}) copy-start(f32[384,2,16]{0,2,1:T(8,128)} %get-tuple-element.7) | copy-start | bytes 147460
  81.0 44.4 %copy-start.8 = (f32[384,2,16]{0,2,1:T(8,128)S(1)}, f32[384,2,16]{0,2,1:T(8,128)}, u32[]{:S(2)}) copy-start(f32[384,2,16]{0,2,1:T(8,128)} %get-tuple-element.8) | copy-start | bytes 147460
  81.0 44.4 %copy-start.9 = (f32[384,2,16]{0,2,1:T(8,128)S(1)}, f32[384,2,16]{0,2,1:T(8,128)}, u32[]{:S(2)}) copy-start(f32[384,2,16]{0,2,1:T(8,128)} %get-tuple-element.9) | copy-start | bytes 147460
  81.0 44.4 %copy-start.10 = (f32[384,2,16]{0,2,1:T(8,128)S(1)}, f32[384,2,16]{0,2,1:T(8,128)}, u32[]{:S(2)}) copy-start(f32[384,2,16]{0,2,1:T(8,128)} %get-tuple-element.10) | copy-start | bytes 147460
  126.3 1.0 copy-start.20
  143.8 1.0 copy-start.2
where the time goes:
time: 159 us
  blocking collectives  129 us (81%)
  matrix products  18.4 us (12%)
  other arithmetic  7.9 us (5%)
  local copies, waits for them, and re-layouts  3.43 us (2%)
    all_gather x1, blocking collectives, on_device(): lax.all_gather(own_nope, 'sp', axis=0, tiled=True)  16.9 us
    all_gather x1, blocking collectives, on_device(): lax.all_gather(own_values, 'sp', axis=0, tiled=True)  15.6 us
    all_gather x1, blocking collectives, on_device(): lax.all_gather(rope_group, 'sp', axis=0, tiled=True)  14.6 us
    all_gather x1, blocking collectives, on_device(): lax.all_gather(context_latent, 'sp', axis=0, tiled=True)  13.8 us
    psum x1, blocking collectives, on_device(): summed = lax.psum(partials, 'sp')  13.8 us
    all_gather x1, blocking collectives, on_device(): lax.all_gather(context_rope, 'sp', axis=0, tiled=True)  12.2 us
    all_gather x1, blocking collectives, on_device(): lax.all_gather(latent_low, 'tp', axis=0, tiled=True)  8.7 us
    all_gather x1, blocking collectives, on_device(): lax.all_gather(query_low, 'tp', axis=0, tiled=True)  8.53 us

commit v1 on v0

--- a/solution.py
+++ b/solution.py
@@ -100,7 +100,7 @@
         ]
     )
     summed = lax.psum(partials, "sp")
-    modulation = lax.all_gather(summed, "tp", axis=1, tiled=True)
+    modulation = jnp.concatenate(lax.all_gather(summed, "tp"), axis=1)
     shift_vec = modulation[0]
     scale_vec = modulation[1]
     gate_vec = modulation[2]

time: 159 us -> 159 us (level)
  no operation moved by 1% of the time
where the time goes in v1:
time: 159 us
  blocking collectives  129 us (81%)
  matrix products  18.4 us (12%)
  other arithmetic  7.9 us (5%)
  local copies, waits for them, and re-layouts  3.43 us (2%)
    all_gather x1, blocking collectives, on_device(): lax.all_gather(own_nope, 'sp', axis=0, tiled=True)  16.9 us
    all_gather x1, blocking collectives, on_device(): lax.all_gather(own_values, 'sp', axis=0, tiled=True)  15.6 us
    all_gather x1, blocking collectives, on_device(): lax.all_gather(rope_group, 'sp', axis=0, tiled=True)  14.6 us
    all_gather x1, blocking collectives, on_device(): lax.all_gather(context_latent, 'sp', axis=0, tiled=True)  13.8 us
    psum x1, blocking collectives, on_device(): summed = lax.psum(partials, 'sp')  13.8 us
    all_gather x1, blocking collectives, on_device(): lax.all_gather(context_rope, 'sp', axis=0, tiled=True)  12.2 us
    all_gather x1, blocking collectives, on_device(): lax.all_gather(latent_low, 'tp', axis=0, tiled=True)  8.7 us
    all_gather x1, blocking collectives, on_device(): lax.all_gather(query_low, 'tp', axis=0, tiled=True)  8.53 us

profile of v1, /device:TPU:0, one launch (start us, length us, event | category | flops | bytes accessed | tf_op | source)
XLA Modules:
  0.0 158.7 jit_solution(15833898411083995222)
XLA Ops:
  0.6 0.7 fusion.54
  1.3 1.2 fusion.72
  2.6 1.2 fusion.73
  3.8 1.3 fusion.74
  5.1 13.8 %psum.7 = f32[1,3,512]{2,1,0:T(4,128)S(1)} all-reduce(f32[1,3,512]{2,1,0:T(4,128)S(1)} %maximum_bitcast_fusion), channel_id=1, replica_groups=mesh['sp'=4,'tp'=4,'dp'=2] {'sp'}, use_global_device_ids=true, to_apply=%region_0.1 | all-reduce | flops 1536 | bytes 12288 | tf_op jit(solution)/shard_map/psum | solution.py:102
  18.9 8.2 %all_gather.31 = f32[4,3,512]{2,1,0:T(4,128)S(1)} all-gather(f32[1,3,512]{2,1,0:T(4,128)S(1)} %psum.7), channel_id=1, replica_groups=mesh['sp'=4,'tp'=4,'dp'=2] {'tp'}, dimensions={0}, use_global_device_ids=true | all-gather | bytes 30720 | tf_op jit(solution)/shard_map/all_gather | solution.py:103
  27.1 1.2 fusion.26
  28.4 1.9 %multiply_reduce_fusion.1 = (f32[96]{0:T(128)S(1)}, f32[96,256]{1,0:T(8,128)S(1)}) fusion(bf16[2048,256]{1,0:T(8,128)(2,1)} %param.27, bf16[96,2048]{1,0:T(8,128)(2,1)} %param.18, f32[2048]{0:T(1024)S(1)} %bitcast.123, f32[2048]{0:T(1024)S(1)} %bitcast.126, f32[2048]{0:T(1024)} %param.25, f32[96]{0:T(128)S(1)} %add_rsqrt_fusion.2), kind=kOutput, calls=%fused_computation.50 | convolution fusion | flops 101892000 | bytes 1565440 | tf_op jit(solution)/shard_map/dot_general | solution.py:115
  30.3 8.7 %all_gather.35 = bf16[384,256]{1,0:T(8,128)(2,1)S(1)} all-gather(bf16[96,256]{1,0:T(8,128)(2,1)S(1)} %multiply_convert_fusion.1), channel_id=1, replica_groups=mesh['sp'=4,'tp'=4,'dp'=2] {'tp'}, dimensions={0}, use_global_device_ids=true | all-gather | bytes 245760 | tf_op jit(solution)/shard_map/all_gather | solution.py:126
  39.1 13.8 %all_gather.33 = bf16[512,256]{1,0:T(8,128)(2,1)S(1)} all-gather(bf16[128,256]{1,0:T(8,128)(2,1)S(1)} %copy-done.12), channel_id=1, replica_groups=mesh['sp'=4,'tp'=4,'dp'=2] {'sp'}, dimensions={0}, use_global_device_ids=true | all-gather | bytes 327680 | tf_op jit(solution)/shard_map/all_gather | solution.py:141
  52.9 0.9 convolution_convert_fusion.3
  54.0 1.0 convolution_convert_fusion
  56.0 8.5 %all_gather.32 = bf16[384,512]{1,0:T(8,128)(2,1)S(1)} all-gather(bf16[96,512]{1,0:T(8,128)(2,1)S(1)} %multiply_convert_fusion), channel_id=1, replica_groups=mesh['sp'=4,'tp'=4,'dp'=2] {'tp'}, dimensions={0}, use_global_device_ids=true | all-gather | bytes 491520 | tf_op jit(solution)/shard_map/all_gather | solution.py:125
  65.0 0.7 slice_negate_fusion.1
  66.3 1.3 fusion.62
  67.6 0.6 copy-done.11
  68.9 0.7 broadcast_multiply_fusion.3
  69.6 0.9 fusion.47
  70.5 8.2 %all-gather = bf16[4,96,64]{1,2,0:T(8,128)(2,1)S(1)} all-gather(bf16[1,96,64]{1,2,0:T(8,128)(2,1)S(1)} %fusion.47), channel_id=1, replica_groups=mesh['sp'=4,'tp'=4,'dp'=2] {'tp'}, dimensions={0}, use_global_device_ids=true | all-gather | bytes 61440 | tf_op jit(solution)/shard_map/all_gather | solution.py:127
  78.7 0.7 copy.48
  79.4 1.6 reshape.272
  81.0 14.6 %all_gather.38 = bf16[1536,64]{0,1:T(8,128)(2,1)S(1)} all-gather(bf16[384,64]{0,1:T(8,128)(2,1)} %reshape.272), channel_id=1, replica_groups=mesh['sp'=4,'tp'=4,'dp'=2] {'sp'}, dimensions={0}, use_global_device_ids=true | all-gather | bytes 245760 | tf_op jit(solution)/shard_map/all_gather | solution.py:194
  95.6 16.9 %all_gather.36 = bf16[1536,256]{1,0:T(8,128)(2,1)S(1)} all-gather(bf16[384,256]{1,0:T(8,128)(2,1)} %convolution_convert_fusion.3), channel_id=1, replica_groups=mesh['sp'=4,'tp'=4,'dp'=2] {'sp'}, dimensions={0}, use_global_device_ids=true | all-gather | bytes 983040 | tf_op jit(solution)/shard_map/all_gather | solution.py:192
  112.9 12.2 %all_gather.34 = bf16[512,64]{0,1:T(8,128)(2,1)S(1)} all-gather(bf16[128,64]{0,1:T(8,128)(2,1)S(1)} %copy-done.13), channel_id=1, replica_groups=mesh['sp'=4,'tp'=4,'dp'=2] {'sp'}, dimensions={0}, use_global_device_ids=true | all-gather | bytes 81920 | tf_op jit(solution)/shard_map/all_gather | solution.py:142
  125.5 0.8 fusion.39
  126.3 1.0 fusion.71
  128.3 15.6 %all_gather.39 = bf16[1536,256]{1,0:T(8,128)(2,1)S(1)} all-gather(bf16[384,256]{1,0:T(8,128)(2,1)S(1)} %convolution_convert_fusion.2), channel_id=1, replica_groups=mesh['sp'=4,'tp'=4,'dp'=2] {'sp'}, dimensions={0}, use_global_device_ids=true | all-gather | bytes 983040 | tf_op jit(solution)/shard_map/all_gather | solution.py:193
  143.9 0.8 fusion.1
  144.8 0.7 fusion.19
  145.5 0.9 fusion.23
  146.8 8.1 %all_to_all.19 = bf16[4,96,256]{2,1,0:T(8,128)(2,1)S(1)} all-to-all(bf16[4,96,256]{2,1,0:T(8,128)(2,1)S(1)} %all_to_all.14), channel_id=1, replica_groups=mesh['sp'=4,'tp'=4,'dp'=2] {'tp'}, dimensions={0} | all-to-all | bytes 393216 | tf_op jit(solution)/shard_map/all_to_all | solution.py:200
  154.9 3.8 %fusion.7 = bf16[96,2048]{1,0:T(8,128)(2,1)} fusion(bf16[96,1024]{1,0:T(8,128)(2,1)S(1)} %bitcast.119, bf16[1024,2048]{1,0:T(8,128)(2,1)} %param.35, bf16[96,2048]{1,0:T(8,128)(2,1)S(1)} %copy-done.1, f32[2048]{0:T(1024)S(1)} %bitcast.122), kind=kOutput, calls=%fused_computation.9 | convolution fusion | flops 403439616 | bytes 5185536 | tf_op jit(solution)/shard_map/dot_general | solution.py:201
  (72 shorter events, 5.8 us)
Async XLA Ops:
  0.0 55.3 %copy-start = (bf16[2048,512]{1,0:T(8,128)(2,1)S(1)}, bf16[2048,512]{1,0:T(8,128)(2,1)}, u32[]{:S(2)}) copy-start(bf16[2048,512]{1,0:T(8,128)(2,1)} %param.26) | copy-start | bytes 6291460
  0.0 30.2 %copy-start.19 = (f32[256]{0:T(256)S(1)}, f32[256]{0:T(256)}, u32[]{:S(2)}) copy-start(f32[256]{0:T(256)} %param.30) | copy-start | bytes 3076
  0.0 39.0 %copy-start.12 = (bf16[128,256]{1,0:T(8,128)(2,1)S(1)}, bf16[128,256]{1,0:T(8,128)(2,1)}, u32[]{:S(2)}) copy-start(bf16[128,256]{1,0:T(8,128)(2,1)} %param.20) | copy-start | bytes 196612
  1.3 51.5 %copy-start.3 = (bf16[256,256]{1,0:T(8,128)(2,1)S(1)}, bf16[256,256]{1,0:T(8,128)(2,1)}, u32[]{:S(2)}) copy-start(bf16[256,256]{1,0:T(8,128)(2,1)} %param.32) | copy-start | bytes 393220
  3.8 50.2 %copy-start.4 = (bf16[256,256]{1,0:T(8,128)(2,1)S(1)}, bf16[256,256]{1,0:T(8,128)(2,1)}, u32[]{:S(2)}) copy-start(bf16[256,256]{1,0:T(8,128)(2,1)} %param.33) | copy-start | bytes 393220
  27.1 28.1 %copy-start.14 = (f32[1,4,512]{2,0,1:T(1,128)}, f32[1,4,512]{2,0,1:T(1,128)S(1)}, u32[]{:S(2)}) copy-start(f32[1,4,512]{2,0,1:T(1,128)S(1)} %get-tuple-element.15) | copy-start | bytes 24580
  27.1 27.9 %copy-start.5 = (bf16[256,256]{1,0:T(8,128)(2,1)S(1)}, bf16[256,256]{1,0:T(8,128)(2,1)}, u32[]{:S(2)}) copy-start(bf16[256,256]{1,0:T(8,128)(2,1)} %param.33) | copy-start | bytes 393220
  28.3 26.9 %copy-start.22 = (f32[96]{0:T(128)}, f32[96]{0:T(128)S(1)}, u32[]{:S(2)}) copy-start(f32[96]{0:T(128)S(1)} %add_rsqrt_fusion.2) | copy-start | bytes 1156
  28.3 26.9 %copy-start.1 = (bf16[96,2048]{1,0:T(8,128)(2,1)S(1)}, bf16[96,2048]{1,0:T(8,128)(2,1)}, u32[]{:S(2)}) copy-start(bf16[96,2048]{1,0:T(8,128)(2,1)} %param.18) | copy-start | bytes 1179652
  28.4 26.9 %copy-start.21 = (f32[2048]{0:T(1024)S(1)}, f32[2048]{0:T(1024)}, u32[]{:S(2)}) copy-start(f32[2048]{0:T(1024)} %param.25) | copy-start | bytes 24580
  53.7 2.2 %copy-start.17 = (f32[512]{0:T(512)S(1)}, f32[512]{0:T(512)}, u32[]{:S(2)}) copy-start(f32[512]{0:T(512)} %param.29) | copy-start | bytes 6148
  54.0 10.5 %copy-start.6 = (bf16[512,384]{1,0:T(8,128)(2,1)S(1)}, bf16[512,384]{1,0:T(8,128)(2,1)}, u32[]{:S(2)}) copy-start(bf16[512,384]{1,0:T(8,128)(2,1)} %param.31) | copy-start | bytes 1179652
  67.6 0.6 copy-start.11
  70.5 54.6 %copy-start.15 = (f32[384]{0:T(512)S(1)}, f32[384]{0:T(512)}, u32[]{:S(2)}) copy-start(f32[384]{0:T(512)} %get-tuple-element.33) | copy-start | bytes 4612
  70.5 54.6 %copy-start.16 = (f32[384]{0:T(512)S(1)}, f32[384]{0:T(512)}, u32[]{:S(2)}) copy-start(f32[384]{0:T(512)} %get-tuple-element.34) | copy-start | bytes 4612
  81.0 31.9 %copy-start.13 = (bf16[128,64]{0,1:T(8,128)(2,1)S(1)}, bf16[128,64]{0,1:T(8,128)(2,1)}, u32[]{:S(2)}) copy-start(bf16[128,64]{0,1:T(8,128)(2,1)} %param.21) | copy-start | bytes 49156
  81.0 44.1 %copy-start.18 = (f32[16]{0:T(128)S(1)}, f32[16]{0:T(128)}, u32[]{:S(2)}) copy-start(f32[16]{0:T(128)} %multiply_power_fusion) | copy-start | bytes 196
  81.0 44.4 %copy-start.7 = (f32[384,2,16]{0,2,1:T(8,128)S(1)}, f32[384,2,16]{0,2,1:T(8,128)}, u32[]{:S(2)}) copy-start(f32[384,2,16]{0,2,1:T(8,128)} %get-tuple-element.7) | copy-start | bytes 147460
  81.0 44.4 %copy-start.8 = (f32[384,2,16]{0,2,1:T(8,128)S(1)}, f32[384,2,16]{0,2,1:T(8,128)}, u32[]{:S(2)}) copy-start(f32[384,2,16]{0,2,1:T(8,128)} %get-tuple-element.8) | copy-start | bytes 147460
  81.0 44.4 %copy-start.9 = (f32[384,2,16]{0,2,1:T(8,128)S(1)}, f32[384,2,16]{0,2,1:T(8,128)}, u32[]{:S(2)}) copy-start(f32[384,2,16]{0,2,1:T(8,128)} %get-tuple-element.9) | copy-start | bytes 147460
  81.0 44.4 %copy-start.10 = (f32[384,2,16]{0,2,1:T(8,128)S(1)}, f32[384,2,16]{0,2,1:T(8,128)}, u32[]{:S(2)}) copy-start(f32[384,2,16]{0,2,1:T(8,128)} %get-tuple-element.10) | copy-start | bytes 147460
  126.3 1.0 copy-start.20
  143.9 1.0 copy-start.2
